TPU v7x, 32 devices: a whole 2x2x4 slice. The times are simulated.
32 devices in a mesh: dp: 4 (over y, x), kv: 4 (over z), tp: 2 (over core).
Axes of the slice: x: 2, y: 2, z: 4, core: 2. Of those that a mesh axis runs over, the one named last changes fastest.
Arguments:
- tokens: bfloat16 [16, 4096], P('dp', 'kv'), may hold values from -24 to 24
- positions: int32 [16], P(('dp', 'kv')), may hold values from 0 to 4095
- state: float32 [16, 16, 128, 128], P(('dp', 'kv'), 'tp'), may hold values from -0.6 to 0.6
- w_query: bfloat16 [4096, 2048], P('kv', 'tp'), may hold values from -0.09375 to 0.09375
- w_key: bfloat16 [4096, 2048], P('kv', 'tp'), may hold values from -0.09375 to 0.09375
- w_value: bfloat16 [4096, 2048], P('kv', 'tp'), may hold values from -0.09375 to 0.09375
- w_gate: bfloat16 [4096, 2048], P('kv', 'tp'), may hold values from -0.09375 to 0.09375
- w_out: bfloat16 [2048, 4096], P(None, ('kv', 'tp')), may hold values from -0.25 to 0.25
- gain_mix: float32 [4096], replicated, may hold values from 0.1 to 1.9
- w_ffn_gate: bfloat16 [4096, 11008], P(None, ('kv', 'tp')), may hold values from -0.09375 to 0.09375
- w_ffn_up: bfloat16 [4096, 11008], P(None, ('kv', 'tp')), may hold values from -0.09375 to 0.09375
- w_ffn_down: bfloat16 [11008, 4096], P(('kv', 'tp')), may hold values from -0.109375 to 0.109375
- gain_out: float32 [4096], replicated, may hold values from 0.1 to 1.9
Outputs:
- layer_out: bfloat16 [16, 4096], P('dp', ('kv', 'tp'))
- new_state: float32 [16, 16, 128, 128], P(('dp', 'kv'), 'tp')
All inputs are finite; a program needn't handle non-finite values.
Results may differ from a plain program's by a relative error of at most 0.018.
Values may be sent and summed in bfloat16 or wider, within the bound.
A program may use at most 128 MiB of HBM per device.

v0:
```python
import jax
import jax.numpy as jnp
from jax import lax
from jax.sharding import PartitionSpec as P


def rotate(vectors, positions):
    half = vectors.shape[-1] // 2
    inverse = 10000.0 ** (-jnp.arange(half, dtype=jnp.float32) / half)
    angle = positions.astype(jnp.float32)[:, None, None] * inverse[None, None, :]
    cosine = jnp.cos(angle)
    sine = jnp.sin(angle)
    first = vectors[..., :half]
    second = vectors[..., half:]
    return jnp.concatenate([first * cosine - second * sine, first * sine + second * cosine], -1)


def finish_norm(values, sums, squares, count, gain):
    mean = sums / count
    var = squares / count - mean * mean
    return (values - mean[:, None]) * lax.rsqrt(var + 1e-05)[:, None] * gain[None, :]


def on_device(
    tokens,
    positions,
    state,
    w_query,
    w_key,
    w_value,
    w_gate,
    w_out,
    gain_mix,
    w_ffn_gate,
    w_ffn_up,
    w_ffn_down,
    gain_out,
):
    seqs = state.shape[0]
    heads = state.shape[1]
    width_head = state.shape[2]
    proj_cols = w_query.shape[1]
    width = w_ffn_gate.shape[0]
    cols = w_out.shape[1]
    group_rows = tokens.shape[0]
    kv_count = lax.axis_size("kv")
    tp_count = lax.axis_size("tp")
    tp_index = lax.axis_index("tp")
    col_start = (lax.axis_index("kv") * tp_count + tp_index) * cols
    projected = lax.psum_scatter(
        jnp.concatenate(
            [
                jnp.dot(tokens, w_query, preferred_element_type=jnp.float32),
                jnp.dot(tokens, w_key, preferred_element_type=jnp.float32),
                jnp.dot(tokens, w_value, preferred_element_type=jnp.float32),
                jnp.dot(tokens, w_gate, preferred_element_type=jnp.float32),
            ],
            axis=1,
        ),
        "kv",
        scatter_dimension=0,
        tiled=True,
    )
    query = projected[:, :proj_cols].reshape(seqs, heads, width_head)
    key = projected[:, proj_cols : 2 * proj_cols].reshape(seqs, heads, width_head)
    value = projected[:, 2 * proj_cols : 3 * proj_cols].reshape(seqs, heads, width_head)
    gate_pre = projected[:, 3 * proj_cols :]
    query = rotate(query, positions)
    key = rotate(key, positions) * width_head ** (-0.5)
    total_heads = heads * tp_count
    head_ids = (tp_index * heads + jnp.arange(heads, dtype=jnp.int32)).astype(jnp.float32)
    decay = 1.0 - 2.0 ** (-5.0 - 6.0 * head_ids / (total_heads - 1))
    new_state = decay[None, :, None, None] * state + key[:, :, :, None] * value[:, :, None, :]
    retained = jnp.einsum("bhd,bhdv->bhv", query, new_state, precision=lax.Precision.HIGHEST)
    mean = jnp.mean(retained, -1, keepdims=True)
    var = jnp.mean(jnp.square(retained - mean), -1, keepdims=True)
    normed = (retained - mean) * lax.rsqrt(var + 1e-05)
    attended = (normed.reshape(seqs, proj_cols) * jax.nn.silu(gate_pre)).astype(jnp.bfloat16)
    gathered = lax.all_gather(attended[None], ("kv", "tp"), axis=0, tiled=True)
    gathered = gathered.reshape(kv_count, tp_count, seqs, proj_cols)
    out_blocks = w_out.reshape(tp_count, proj_cols, cols)
    mixed = jnp.einsum(
        "itsc,tcd->isd", gathered, out_blocks, preferred_element_type=jnp.float32
    ).reshape(group_rows, cols)
    tokens_own = lax.dynamic_slice_in_dim(tokens, tp_index * cols, cols, 1)
    mixed_pre = (tokens_own.astype(jnp.float32) + mixed).astype(jnp.bfloat16)
    gain_out_own = lax.dynamic_slice_in_dim(gain_out, col_start, cols, 0)
    whole_rows = lax.all_gather(mixed_pre, ("kv", "tp"), axis=1, tiled=True).astype(jnp.float32)
    hidden = finish_norm(
        whole_rows, jnp.sum(whole_rows, 1), jnp.sum(whole_rows * whole_rows, 1), width, gain_mix
    ).astype(jnp.bfloat16)
    hidden_own = lax.dynamic_slice_in_dim(hidden, col_start, cols, 1)
    gate = jnp.dot(hidden, w_ffn_gate, preferred_element_type=jnp.float32)
    upward = jnp.dot(hidden, w_ffn_up, preferred_element_type=jnp.float32)
    inner = (jax.nn.silu(gate) * upward).astype(jnp.bfloat16)
    ffn_cols = lax.psum_scatter(
        lax.dot_general(
            w_ffn_down, inner, (((0,), (1,)), ((), ())), preferred_element_type=jnp.float32
        ),
        ("kv", "tp"),
        scatter_dimension=0,
        tiled=True,
    )
    summed = hidden_own.astype(jnp.float32) + ffn_cols.T
    out_sums, out_squares = lax.psum(
        (jnp.sum(summed, 1), jnp.sum(summed * summed, 1)), ("kv", "tp")
    )
    layer_out = finish_norm(summed, out_sums, out_squares, width, gain_out_own).astype(jnp.bfloat16)
    return (layer_out, new_state)


def solution(mesh):
    return jax.shard_map(
        on_device,
        mesh=mesh,
        in_specs=(
            P("dp", "kv"),
            P(("dp", "kv")),
            P(("dp", "kv"), "tp", None, None),
            P("kv", "tp"),
            P("kv", "tp"),
            P("kv", "tp"),
            P("kv", "tp"),
            P(None, ("kv", "tp")),
            P(),
            P(None, ("kv", "tp")),
            P(None, ("kv", "tp")),
            P(("kv", "tp"), None),
            P(),
        ),
        out_specs=(P("dp", ("kv", "tp")), P(("dp", "kv"), "tp", None, None)),
        check_vma=False,
    )
```

profile of v0, /device:TPU:0, one launch (start us, length us, event | category | flops | bytes accessed | tf_op | source)
XLA Modules:
  0.0 164.0 jit_solution(9158389802632589217)
XLA Ops:
  7.3 2.1 %fusion.20 = f32[4,1024]{1,0:T(4,128)S(1)} fusion(bf16[4,1024]{1,0:T(4,128)(2,1)} %param.13, bf16[1024,1024]{1,0:T(8,128)(2,1)} %param.16), kind=kOutput, calls=%fused_computation.51 | convolution fusion | flops 8388608 | bytes 2121728 | tf_op jit(solution)/shard_map/dot_general | solution.py:53
  9.4 0.2 copy-done.1
  9.6 0.4 fusion.21
  10.0 0.2 copy-done.2
  10.2 0.4 fusion.22
  10.6 0.8 copy-done.3
  11.4 0.4 fusion.23
  11.8 0.6 pad_maximum_fusion
  13.2 0.6 dynamic-slice
  13.8 35.8 %all-reduce.4.cloned.1.call-done = f32[4,4096]{1,0:T(4,128)} async-done(((f32[4,4096]{1,0:T(4,128)}), f32[4,4096]{1,0:T(4,128)}) %all-reduce.4.cloned.1.call-update) | async-done | bytes 65552
  49.6 1.5 fusion.19
  51.2 0.1 maximum_multiply_fusion
  51.4 0.2 multiply_add_fusion
  51.6 0.5 fusion.3
  52.1 0.1 reduce_sum.54
  52.3 0.2 multiply_reduce_fusion.1
  52.5 1.5 convert_bitcast_fusion
  54.0 14.1 %all-gather.1 = bf16[8,1,1024]{2,1,0:T(2,128)(2,1)S(1)} all-gather(bf16[1,1,1024]{2,1,0:T(2,128)(2,1)S(1)} %convert_bitcast_fusion), channel_id=2, replica_groups=mesh['dp'=4,'kv'=4,'tp'=2] {'kv','tp'}, dimensions={0}, use_global_device_ids=true | all-gather | bytes 18432 | tf_op jit(solution)/shard_map/all_gather | solution.py:79
  68.1 0.1 reduce.4
  68.2 0.4 fusion.2
  68.6 14.1 %all_gather.7 = bf16[4,4096]{1,0:T(4,128)(2,1)S(1)} all-gather(bf16[4,512]{1,0:T(4,128)(2,1)S(1)} %fusion.2), channel_id=1, replica_groups=mesh['dp'=4,'kv'=4,'tp'=2] {'kv','tp'}, dimensions={1}, use_global_device_ids=true | all-gather | bytes 36864 | tf_op jit(solution)/shard_map/all_gather | solution.py:88
  82.7 0.2 convert_reduce_fusion
  82.9 0.1 fusion.7
  83.0 7.2 %fusion.24 = f32[4,1376]{1,0:T(4,128)S(1)} fusion(bf16[4,4096]{1,0:T(4,128)(2,1)S(1)} %fusion.7, bf16[4096,1376]{0,1:T(8,128)(2,1)} %param.22), kind=kOutput, calls=%fused_computation.55 | convolution fusion | flops 45088768 | bytes 11326976 | tf_op jit(solution)/shard_map/dot_general | solution.py:93
  90.2 12.5 %convolution_bitcast_fusion = f32[4096,4]{0,1:T(4,128)S(1)} fusion(bf16[1376,4096]{1,0:T(8,128)(2,1)} %param.24, bf16[4,4096]{1,0:T(4,128)(2,1)S(1)} %fusion.7, bf16[4096,1376]{0,1:T(8,128)(2,1)} %param.23, f32[4,1376]{1,0:T(4,128)S(1)} %fusion.24), kind=kOutput, calls=%fused_computation | convolution fusion | flops 90210560 | bytes 22664704 | tf_op jit(solution)/shard_map/dot_general | solution.py:97
  102.7 2.0 %copy.19 = f32[4096,4]{1,0:T(8,128)} copy(f32[4096,4]{0,1:T(4,128)S(1)} %convolution_bitcast_fusion) | data formatting | bytes 131072
  104.8 0.8 dynamic_slice.11
  105.5 35.0 %reduce-scatter.4.cloned.1.call-done = f32[512,4]{1,0:T(8,128)} async-done(((f32[4096,4]{1,0:T(8,128)}), f32[512,4]{1,0:T(8,128)}) %reduce-scatter.4.cloned.1.call-update) | async-done | bytes 8208
  140.6 1.1 copy.20
  141.6 0.2 fusion.18
  141.8 14.7 %all-reduce.1 = (f32[4]{0:T(128)S(1)}, f32[4]{0:T(128)S(1)}) all-reduce(f32[4]{0:T(128)S(1)} %get-tuple-element.3, f32[4]{0:T(128)S(1)} %get-tuple-element.2), channel_id=1, replica_groups=mesh['dp'=4,'kv'=4,'tp'=2] {'kv','tp'}, use_global_device_ids=true, to_apply=%region_9.10 | all-reduce | flops 8 | bytes 64 | tf_op jit(solution)/shard_map/psum | solution.py:105
  156.5 0.7 multiply_convert_fusion
  (29 shorter events, 0.5 us)
Async XLA Ops:
  7.2 61.1 %copy-start = (bf16[2048,512]{1,0:T(8,128)(2,1)S(1)}, bf16[2048,512]{1,0:T(8,128)(2,1)}, u32[]{:S(2)}) copy-start(bf16[2048,512]{1,0:T(8,128)(2,1)} %param.20) | copy-start | bytes 6291460
  7.2 2.2 %copy-start.6 = (bf16[4,1024]{1,0:T(4,128)(2,1)S(1)}, bf16[4,1024]{1,0:T(4,128)(2,1)}, u32[]{:S(2)}) copy-start(bf16[4,1024]{1,0:T(4,128)(2,1)} %param.13) | copy-start | bytes 24580
  7.2 42.4 %all-reduce.4.cloned.1.call-start = ((), (), s32[]{:S(2)}) async-start(), calls=%async_computation.2 | async-start | bytes 131072
  7.2 2.3 %copy-start.1 = (bf16[1024,1024]{1,0:T(8,128)(2,1)S(1)}, bf16[1024,1024]{1,0:T(8,128)(2,1)}, u32[]{:S(2)}) copy-start(bf16[1024,1024]{1,0:T(8,128)(2,1)} %param.17) | copy-start | bytes 6291460
  7.2 3.0 %copy-start.2 = (bf16[1024,1024]{1,0:T(8,128)(2,1)S(1)}, bf16[1024,1024]{1,0:T(8,128)(2,1)}, u32[]{:S(2)}) copy-start(bf16[1024,1024]{1,0:T(8,128)(2,1)} %param.18) | copy-start | bytes 6291460
  9.6 1.8 %copy-start.3 = (bf16[1024,1024]{1,0:T(8,128)(2,1)S(1)}, bf16[1024,1024]{1,0:T(8,128)(2,1)}, u32[]{:S(2)}) copy-start(bf16[1024,1024]{1,0:T(8,128)(2,1)} %param.19) | copy-start | bytes 6291460
  10.2 3.0 %copy-start.8 = (u32[32]{0:T(128)S(1)}, u32[32]{0:T(128)}, u32[]{:S(2)}) copy-start(u32[32]{0:T(128)} %constant.61) | copy-start | bytes 388
  10.2 41.2 %copy-start.5 = (f32[1,8,128,128]{3,2,1,0:T(8,128)S(1)}, f32[1,8,128,128]{3,2,1,0:T(8,128)}, u32[]{:S(2)}) copy-start(f32[1,8,128,128]{3,2,1,0:T(8,128)} %param.15) | copy-start | bytes 1572868
  12.4 70.5 %copy-start.7 = (f32[4096]{0:T(1024)S(1)}, f32[4096]{0:T(1024)}, u32[]{:S(2)}) copy-start(f32[4096]{0:T(1024)} %param.21) | copy-start | bytes 49156
  12.4 128.1 %reduce-scatter.4.cloned.1.call-start = ((), (), s32[]{:S(2)}) async-start(), calls=%async_computation.1 | async-start | bytes 2359296
  51.6 38.6 %copy-start.4 = (f32[1,8,128,128]{3,2,1,0:T(8,128)}, f32[1,8,128,128]{3,2,1,0:T(8,128)S(1)}, u32[]{:S(2)}) copy-start(f32[1,8,128,128]{3,2,1,0:T(8,128)S(1)} %multiply_add_fusion) | copy-start | bytes 1572868
Sparse Core Ops, SparseCore 0:
  12.6 37.0 all-reduce.3
  104.9 35.6 reduce-scatter.3
where the time goes:
time: 164 us
  waiting for transfers between devices  70.8 us (43%)
  blocking collectives  42.9 us (26%)
  matrix products  23.9 us (15%)
  between operations  14.8 us (9%)
  local copies, waits for them, and re-layouts  7.22 us (4%)
  other arithmetic  4.24 us (3%)
    unnamed x4, waiting for transfers between devices  70.8 us
    psum x1, blocking collectives, on_device(): lax.psum((jnp.sum(summed, 1), jnp.sum(summed * summed, 1)), ('kv', 'tp'))  14.7 us
    all_gather x1, blocking collectives, on_device(): gathered = lax.all_gather(attended[None], ('kv', 'tp'), axis=0, tiled=True)  14.1 us
    all_gather x1, blocking collectives, on_device(): lax.all_gather(mixed_pre, ('kv', 'tp'), axis=1, tiled=True)  14.1 us
    dot_general x1, matrix products, on_device(): lax.dot_general(w_ffn_down, inner, (((0,), (1,)), ((), ())), preferred_el...  12.5 us
    dot_general x1, matrix products, on_device(): gate = jnp.dot(hidden, w_ffn_gate, preferred_element_type=jnp.float32)  7.2 us
    unnamed x21, local copies, waits for them, and re-layouts  4.91 us
  transfers between devices with their start and end apart: 2, of which 2 were waited for; matrix products, arithmetic and copies ran while one was open for 1% of the time, Pallas kernels for 0%

commit v1 on v0

--- a/solution.py
+++ b/solution.py
@@ -1,7 +1,399 @@
+import functools
+
 import jax
 import jax.numpy as jnp
+import numpy as np
 from jax import lax
+from jax.experimental import pallas as pl
+from jax.experimental.pallas import tpu as pltpu
 from jax.sharding import PartitionSpec as P
+
+MESH = pl.DeviceIdType.MESH
+F32 = jnp.float32
+BF16 = jnp.bfloat16
+
+
+def dot_rows(values, weight):
+    return lax.dot_general(values, weight, (((1,), (1,)), ((), ())), preferred_element_type=F32)
+
+
+def step_kernel(
+    kv_count,
+    tp_count,
+    tok_h,
+    pos_s,
+    state_h,
+    wq_h,
+    wk_h,
+    wv_h,
+    wg_h,
+    wout_h,
+    gmix_h,
+    wfg_h,
+    wfu_h,
+    wfd_h,
+    gout_h,
+    inv_h,
+    out_v,
+    nst_h,
+    tok,
+    state,
+    nst,
+    wq,
+    wk,
+    wv,
+    wg,
+    wout,
+    gmix,
+    wfg,
+    wfu,
+    wfd,
+    gout,
+    inv,
+    qsend,
+    qrecv,
+    att,
+    mix,
+    hid_own,
+    hid,
+    inner,
+    fsend,
+    frecv,
+    sums,
+    local_sem,
+    q_send_sem,
+    q_recv_sem,
+    send_sem,
+    recv_sem,
+):
+    group = kv_count * tp_count
+    dp = lax.axis_index("dp")
+    kv = lax.axis_index("kv")
+    tp = lax.axis_index("tp")
+    me = kv * tp_count + tp
+    rows = tok.shape[0]
+    heads = state.shape[0]
+    width_head = state.shape[1]
+    width = hid.shape[1]
+    cols = mix.shape[2]
+    ff = wfg.shape[0]
+
+    far = sorted(range(1, kv_count), key=lambda d: -min(d, kv_count - d))
+    steps = [(d, e) for d in far for e in range(tp_count)]
+    steps += [(0, e) for e in range(1, tp_count)]
+
+    def partner(d, e):
+        return lax.rem(kv + d, kv_count), lax.rem(tp + e, tp_count)
+
+    barrier = pltpu.get_barrier_semaphore()
+    for d, e in steps:
+        other_kv, other_tp = partner(d, e)
+        pl.semaphore_signal(
+            barrier, inc=1, device_id=(dp, other_kv, other_tp), device_id_type=MESH
+        )
+
+    loads = []
+
+    def load(src, dst):
+        copy = pltpu.make_async_copy(src, dst, local_sem.at[len(loads)])
+        copy.start()
+        loads.append(copy)
+        return copy
+
+    tok_load = load(tok_h, tok)
+    inv_load = load(inv_h, inv)
+    proj_loads = [
+        load(src, dst) for src, dst in ((wq_h, wq), (wk_h, wk), (wv_h, wv), (wg_h, wg))
+    ]
+    state_load = load(state_h, state)
+    gmix_load = load(gmix_h, gmix)
+    gout_load = load(gout_h, gout)
+
+    inv_load.wait()
+    lane = lax.broadcasted_iota(jnp.int32, (1, width_head), 1)
+    angle = pos_s[0].astype(F32) * inv[...]
+    cosine = jnp.cos(angle)
+    sine = jnp.sin(angle)
+    sine = jnp.where(lane < width_head // 2, -sine, sine)
+
+    tok_load.wait()
+    pl.semaphore_wait(barrier, group - 1)
+    later = []
+    q_copies = []
+    for p, weight in enumerate((wq, wk, wv, wg)):
+        proj_loads[p].wait()
+        if p == 0:
+            later.append(load(wout_h, wout))
+        elif p == 1:
+            later.append(load(wfg_h, wfg))
+        elif p == 2:
+            later.append(load(wfu_h, wfu))
+        else:
+            later.append(load(wfd_h, wfd))
+        part = jnp.dot(tok[...], weight[...], preferred_element_type=F32)
+        for i in range(kv_count):
+            for h in range(heads):
+                qsend[i, p, h : h + 1, :] = part[
+                    i : i + 1, h * width_head : (h + 1) * width_head
+                ]
+        for d in far:
+            other_kv, _ = partner(d, 0)
+            copy = pltpu.make_async_remote_copy(
+                src_ref=qsend.at[other_kv, p],
+                dst_ref=qrecv.at[kv, p],
+                send_sem=q_send_sem.at[p, d],
+                recv_sem=q_recv_sem.at[p, d],
+                device_id=(dp, other_kv, tp),
+                device_id_type=MESH,
+            )
+            copy.start()
+            q_copies.append((p, d, copy))
+    wout_load, wfg_load, wfu_load, wfd_load = later
+
+    head_id = (tp * heads + lax.broadcasted_iota(jnp.int32, (heads, width_head), 0)).astype(F32)
+    total_heads = heads * tp_count
+    decay = 1.0 - jnp.exp2(-5.0 - 6.0 * head_id / (total_heads - 1))
+
+    def rotate_row(x):
+        return x * cosine + pltpu.roll(x, width_head // 2, 1) * sine
+
+    projected = []
+    for p in range(4):
+        total = qsend[kv, p]
+        for q, d, copy in q_copies:
+            if q == p:
+                copy.wait_recv()
+                total = total + qrecv[lax.rem(kv + kv_count - d, kv_count), p]
+        projected.append(total)
+    query, key, value, gate_pre = projected
+    query = rotate_row(query)
+    key = rotate_row(key) * width_head ** (-0.5)
+    query_t = jnp.transpose(query)
+    key_t = jnp.transpose(key)
+    state_load.wait()
+    retained = []
+    for h in range(heads):
+        new = decay[h : h + 1, :] * state[h] + key_t[:, h : h + 1] * value[h : h + 1, :]
+        nst[h] = new
+        retained.append(jnp.sum(query_t[:, h : h + 1] * new, axis=0, keepdims=True))
+    retained = jnp.concatenate(retained, axis=0)
+    mean = jnp.mean(retained, -1, keepdims=True)
+    var = jnp.mean(jnp.square(retained - mean), -1, keepdims=True)
+    normed = (retained - mean) * lax.rsqrt(var + 1e-05)
+    silu_gate = gate_pre / (1.0 + jnp.exp(-gate_pre))
+    attended = (normed * silu_gate).astype(BF16).astype(F32)
+    own_rows = pl.ds(pl.multiple_of(me * heads, heads), heads)
+    att[own_rows, :] = attended
+
+    def send_all(phase, src, dst):
+        copies = []
+        for d, e in steps:
+            other_kv, other_tp = partner(d, e)
+            copy = pltpu.make_async_remote_copy(
+                src_ref=src,
+                dst_ref=dst,
+                send_sem=send_sem.at[phase, d * tp_count + e],
+                recv_sem=recv_sem.at[phase, d * tp_count + e],
+                device_id=(dp, other_kv, other_tp),
+                device_id_type=MESH,
+            )
+            copy.start()
+            copies.append(copy)
+        return copies
+
+    att_copies = send_all(0, att.at[own_rows, :], att.at[own_rows, :])
+    nst_store = pltpu.make_async_copy(nst, nst_h, local_sem.at[len(loads)])
+    nst_store.start()
+
+    wout_load.wait()
+    for copy in att_copies:
+        copy.wait_recv()
+    lhs = jnp.concatenate(
+        [
+            att[pl.ds(t * heads + h, rows, stride=tp_count * heads), :]
+            for t in range(tp_count)
+            for h in range(heads)
+        ],
+        axis=1,
+    ).astype(BF16)
+    mixed = jnp.dot(lhs, wout[...], preferred_element_type=F32)
+    tok_own = tok[:, pl.ds(pl.multiple_of(tp * cols, cols), cols)]
+    mix[me] = (tok_own.astype(F32) + mixed).astype(BF16).astype(F32)
+    mix_copies = send_all(1, mix.at[me], mix.at[me])
+    gmix_load.wait()
+    gout_load.wait()
+    for copy in mix_copies:
+        copy.wait_recv()
+    whole = [mix[p] for p in range(group)]
+    total = functools.reduce(lambda a, b: a + b, whole)
+    squares = functools.reduce(lambda a, b: a + b, [x * x for x in whole])
+    mean = jnp.sum(total, 1, keepdims=True) / width
+    var = jnp.sum(squares, 1, keepdims=True) / width - mean * mean
+    scale = lax.rsqrt(var + 1e-05)
+    for p in range(group):
+        block = slice(p * cols, (p + 1) * cols)
+        hidden = ((whole[p] - mean) * scale * gmix[:, block]).astype(BF16)
+        hid[:, block] = hidden
+        hid_own[p] = hidden.astype(F32)
+
+    wfg_load.wait()
+    wfu_load.wait()
+    tile = 256
+    whole_tiles = ff // tile
+
+    def inner_block(at):
+        gate = dot_rows(hid[...], wfg[at, :])
+        upward = dot_rows(hid[...], wfu[at, :])
+        inner[:, at] = (gate / (1.0 + jnp.exp(-gate)) * upward).astype(BF16)
+
+    @pl.loop(0, whole_tiles)
+    def _(j):
+        inner_block(pl.ds(pl.multiple_of(j * tile, tile), tile))
+
+    if ff % tile:
+        inner_block(pl.ds(whole_tiles * tile, ff % tile))
+
+    wfd_load.wait()
+    main = ff // 128 * 128
+
+    def down_block(owner):
+        at = pl.ds(pl.multiple_of(owner * cols, cols), cols)
+        result = jnp.dot(inner[:, :main], wfd[:main, at], preferred_element_type=F32)
+        if main < ff:
+            result += jnp.dot(inner[:, main:], wfd[main:, at], preferred_element_type=F32)
+        return result
+
+    f_copies = []
+    for d, e in steps:
+        other_kv, other_tp = partner(d, e)
+        owner = other_kv * tp_count + other_tp
+        fsend[owner] = down_block(owner)
+        copy = pltpu.make_async_remote_copy(
+            src_ref=fsend.at[owner],
+            dst_ref=frecv.at[me],
+            send_sem=send_sem.at[2, d * tp_count + e],
+            recv_sem=recv_sem.at[2, d * tp_count + e],
+            device_id=(dp, other_kv, other_tp),
+            device_id_type=MESH,
+        )
+        copy.start()
+        f_copies.append((d, e, copy))
+    summed = hid_own[me] + down_block(me)
+    for d, e, copy in f_copies:
+        copy.wait_recv()
+        source = lax.rem(kv + kv_count - d, kv_count) * tp_count + lax.rem(
+            tp + tp_count - e, tp_count
+        )
+        summed = summed + frecv[source]
+    own_sum = jnp.sum(summed, 1, keepdims=True)
+    own_square = jnp.sum(summed * summed, 1, keepdims=True)
+    sums[me, 0] = jnp.broadcast_to(own_sum, (rows, 128))
+    sums[me, 1] = jnp.broadcast_to(own_square, (rows, 128))
+    sum_copies = send_all(3, sums.at[me], sums.at[me])
+    for copy in sum_copies:
+        copy.wait_recv()
+    all_sum = functools.reduce(lambda a, b: a + b, [sums[p, 0] for p in range(group)])
+    all_square = functools.reduce(lambda a, b: a + b, [sums[p, 1] for p in range(group)])
+    mean = all_sum[:, :1] / width
+    var = all_square[:, :1] / width - mean * mean
+    gain = gout[:, pl.ds(pl.multiple_of(me * cols, cols), cols)]
+    out_v[...] = ((summed - mean) * lax.rsqrt(var + 1e-05) * gain).astype(BF16)
+
+    for _, _, copy in q_copies:
+        copy.wait_send()
+    for copies in (att_copies, mix_copies, sum_copies):
+        for copy in copies:
+            copy.wait_send()
+    for _, _, copy in f_copies:
+        copy.wait_send()
+    nst_store.wait()
+
+
+def fused_step(
+    tokens,
+    positions,
+    state,
+    w_query,
+    w_key,
+    w_value,
+    w_gate,
+    w_out,
+    gain_mix,
+    w_ffn_gate,
+    w_ffn_up,
+    w_ffn_down,
+    gain_out,
+):
+    kv_count = lax.axis_size("kv")
+    tp_count = lax.axis_size("tp")
+    group = kv_count * tp_count
+    rows = tokens.shape[0]
+    _, heads, width_head, _ = state.shape
+    width = w_ffn_gate.shape[0]
+    cols = w_out.shape[1]
+    half = width_head // 2
+    inverse = 10000.0 ** (-np.arange(half, dtype=np.float32) / half)
+    inverse = np.tile(inverse.astype(np.float32), 2)[None, :]
+    arrays = (
+        tokens,
+        state[0],
+        w_query,
+        w_key,
+        w_value,
+        w_gate,
+        w_out,
+        gain_mix[None, :],
+        w_ffn_gate.T,
+        w_ffn_up.T,
+        w_ffn_down,
+        gain_out[None, :],
+        jnp.asarray(inverse),
+    )
+    held = [pltpu.VMEM(a.shape, a.dtype) for a in arrays]
+    held.insert(2, pltpu.VMEM(arrays[1].shape, F32))
+    any_spec = pl.BlockSpec(memory_space=pl.ANY)
+    out, new_state = pl.pallas_call(
+        functools.partial(step_kernel, kv_count, tp_count),
+        out_shape=(
+            jax.ShapeDtypeStruct((rows, cols), BF16),
+            jax.ShapeDtypeStruct(arrays[1].shape, F32),
+        ),
+        in_specs=[any_spec, pl.BlockSpec(memory_space=pltpu.SMEM)] + [any_spec] * 12,
+        out_specs=(pl.BlockSpec(memory_space=pltpu.VMEM), any_spec),
+        scratch_shapes=held
+        + [
+            pltpu.VMEM((kv_count, 4, heads, width_head), F32),
+            pltpu.VMEM((kv_count, 4, heads, width_head), F32),
+            pltpu.VMEM((group * heads, width_head), F32),
+            pltpu.VMEM((group, rows, cols), F32),
+            pltpu.VMEM((group, rows, cols), F32),
+            pltpu.VMEM((rows, width), BF16),
+            pltpu.VMEM((rows, w_ffn_gate.shape[1]), BF16),
+            pltpu.VMEM((group, rows, cols), F32),
+            pltpu.VMEM((group, rows, cols), F32),
+            pltpu.VMEM((group, 2, rows, 128), F32),
+            pltpu.SemaphoreType.DMA((len(arrays) + 1,)),
+            pltpu.SemaphoreType.DMA((4, kv_count)),
+            pltpu.SemaphoreType.DMA((4, kv_count)),
+            pltpu.SemaphoreType.DMA((4, group)),
+            pltpu.SemaphoreType.DMA((4, group)),
+        ],
+        compiler_params=pltpu.CompilerParams(
+            collective_id=0, has_side_effects=True, vmem_limit_bytes=60 * 1024 * 1024
+        ),
+    )(arrays[0], positions, *arrays[1:])
+    return out, new_state[None]
+
+
+def fits_kernel(tokens, state, w_out, kv_count, tp_count):
+    seqs, _, width_head, _ = state.shape
+    return (
+        seqs == 1
+        and width_head == 128
+        and w_out.shape[1] % 128 == 0
+        and tokens.shape[0] == kv_count
+        and kv_count * tp_count <= 16
+    )
 
 
 def rotate(vectors, positions):
@@ -36,6 +428,22 @@
     w_ffn_down,
     gain_out,
 ):
+    if fits_kernel(tokens, state, w_out, lax.axis_size("kv"), lax.axis_size("tp")):
+        return fused_step(
+            tokens,
+            positions,
+            state,
+            w_query,
+            w_key,
+            w_value,
+            w_gate,
+            w_out,
+            gain_mix,
+            w_ffn_gate,
+            w_ffn_up,
+            w_ffn_down,
+            gain_out,
+        )
     seqs = state.shape[0]
     heads = state.shape[1]
     width_head = state.shape[2]

time: 164 us -> 41.1 us (0.25)
  waiting for transfers between devices: 70.8 us -> 0 us
  blocking collectives: 42.9 us -> 0 us
  Pallas kernels: 0 us -> 36.4 us
  matrix products: 23.9 us -> 0 us
  between operations: 14.8 us -> 1.29 us
  other arithmetic: 4.24 us -> 0 us
  local copies, waits for them, and re-layouts: 7.22 us -> 3.14 us
    unnamed x4 -> x0, waiting for transfers between devices: 70.8 us -> none
    pallas_call x0 -> x1, Pallas kernels: none -> 36.4 us  [fused_step(): pl.pallas_call(functools.partial(step_kernel, kv_count, tp_count), out_sh...]
    all_gather x2 -> x0, blocking collectives: 28.2 us -> none  [the longest x1 14.1 us: on_device(): gathered = lax.all_gather(attended[None], ('kv', 'tp'), axis=0, tiled=True)]
    dot_general x8 -> x0, matrix products: 23.9 us -> none  [the longest x1 12.5 us: on_device(): lax.dot_general(w_ffn_down, inner, (((0,), (1,)), ((), ())), preferred_el...]
    psum x1 -> x0, blocking collectives: 14.7 us -> none  [on_device(): lax.psum((jnp.sum(summed, 1), jnp.sum(summed * summed, 1)), ('kv', 'tp'))]
    unnamed x21 -> x2, local copies, waits for them, and re-layouts: 4.91 us -> 3.14 us
  transfers between devices with their start and end apart: 2 -> 0, of which waited for: 2 -> 0; matrix products, arithmetic and copies ran while one was open for 1% -> 0% of each run, Pallas kernels for 0% -> 0%
where the time goes in v1:
time: 41.1 us; the launch traced here: 40.8 us
  Pallas kernels  36.4 us (89%)
  local copies, waits for them, and re-layouts  3.14 us (8%)
  between operations  1.29 us (3%)
    pallas_call x1, Pallas kernels, fused_step(): pl.pallas_call(functools.partial(step_kernel, kv_count, tp_count), out_sh...  36.4 us
    unnamed x2, local copies, waits for them, and re-layouts  3.14 us

profile of v1, /device:TPU:0, one launch (start us, length us, event | category | flops | bytes accessed | tf_op | source)
XLA Modules:
  0.0 40.8 jit_solution(9821340677854237567)
XLA Ops:
  1.3 36.4 %shard_map.149 = (bf16[4,512]{1,0:T(4,128)(2,1)}, f32[8,128,128]{2,1,0:T(8,128)}) custom-call(bf16[4,1024]{1,0:T(4,128)(2,1)} %tok_h.1, s32[1]{0:T(128)S(6)} %copy.18.pos_s, f32[8,128,128]{2,1,0:T(8,128)} %bitcast.8, bf16[1024,1024]{1,0:T(8,128)(2,1)} %wq_h.1, bf16[1024,1024]{1,0:T(8,128)(2,1)} %wk_h.1, bf16[1024,1024]{1,0:T(8,128)(2,1)} %wv_h.1, ...), custom_call_target="tpu_custom_call" | custom-call | tf_op jit(solution)/shard_map/pallas_call | solution.py:355
  37.7 1.3 %copy.19 = bf16[4,512]{1,0:T(4,128)(2,1)} copy(bf16[4,512]{1,0:T(4,128)(2,1)} %get-tuple-element.8) | data formatting | bytes 8192
  39.0 1.9 %copy.20 = f32[1,8,128,128]{3,2,1,0:T(8,128)} copy(f32[1,8,128,128]{3,2,1,0:T(8,128)} %bitcast.9) | data formatting | bytes 1048576

commit v2 on v1

--- a/solution.py
+++ b/solution.py
@@ -21,7 +21,7 @@
     kv_count,
     tp_count,
     tok_h,
-    pos_s,
+    pos_h,
     state_h,
     wq_h,
     wk_h,
@@ -35,10 +35,10 @@
     gout_h,
     inv_h,
     out_v,
-    nst_h,
+    nst,
     tok,
+    pos,
     state,
-    nst,
     wq,
     wk,
     wv,
@@ -101,6 +101,7 @@
         return copy
 
     tok_load = load(tok_h, tok)
+    pos_load = load(pos_h, pos)
     inv_load = load(inv_h, inv)
     proj_loads = [
         load(src, dst) for src, dst in ((wq_h, wq), (wk_h, wk), (wv_h, wv), (wg_h, wg))
@@ -109,9 +110,10 @@
     gmix_load = load(gmix_h, gmix)
     gout_load = load(gout_h, gout)
 
+    pos_load.wait()
     inv_load.wait()
     lane = lax.broadcasted_iota(jnp.int32, (1, width_head), 1)
-    angle = pos_s[0].astype(F32) * inv[...]
+    angle = pos[...].astype(F32) * inv[...]
     cosine = jnp.cos(angle)
     sine = jnp.sin(angle)
     sine = jnp.where(lane < width_head // 2, -sine, sine)
@@ -202,8 +204,6 @@
         return copies
 
     att_copies = send_all(0, att.at[own_rows, :], att.at[own_rows, :])
-    nst_store = pltpu.make_async_copy(nst, nst_h, local_sem.at[len(loads)])
-    nst_store.start()
 
     wout_load.wait()
     for copy in att_copies:
@@ -218,13 +218,13 @@
     ).astype(BF16)
     mixed = jnp.dot(lhs, wout[...], preferred_element_type=F32)
     tok_own = tok[:, pl.ds(pl.multiple_of(tp * cols, cols), cols)]
-    mix[me] = (tok_own.astype(F32) + mixed).astype(BF16).astype(F32)
+    mix[me] = (tok_own.astype(F32) + mixed).astype(BF16)
     mix_copies = send_all(1, mix.at[me], mix.at[me])
     gmix_load.wait()
     gout_load.wait()
     for copy in mix_copies:
         copy.wait_recv()
-    whole = [mix[p] for p in range(group)]
+    whole = [mix[p].astype(F32) for p in range(group)]
     total = functools.reduce(lambda a, b: a + b, whole)
     squares = functools.reduce(lambda a, b: a + b, [x * x for x in whole])
     mean = jnp.sum(total, 1, keepdims=True) / width
@@ -246,9 +246,8 @@
         upward = dot_rows(hid[...], wfu[at, :])
         inner[:, at] = (gate / (1.0 + jnp.exp(-gate)) * upward).astype(BF16)
 
-    @pl.loop(0, whole_tiles)
-    def _(j):
-        inner_block(pl.ds(pl.multiple_of(j * tile, tile), tile))
+    for j in range(whole_tiles):
+        inner_block(pl.ds(j * tile, tile))
 
     if ff % tile:
         inner_block(pl.ds(whole_tiles * tile, ff % tile))
@@ -267,7 +266,7 @@
     for d, e in steps:
         other_kv, other_tp = partner(d, e)
         owner = other_kv * tp_count + other_tp
-        fsend[owner] = down_block(owner)
+        fsend[owner] = down_block(owner).astype(BF16)
         copy = pltpu.make_async_remote_copy(
             src_ref=fsend.at[owner],
             dst_ref=frecv.at[me],
@@ -284,18 +283,17 @@
         source = lax.rem(kv + kv_count - d, kv_count) * tp_count + lax.rem(
             tp + tp_count - e, tp_count
         )
-        summed = summed + frecv[source]
+        summed = summed + frecv[source].astype(F32)
     own_sum = jnp.sum(summed, 1, keepdims=True)
     own_square = jnp.sum(summed * summed, 1, keepdims=True)
-    sums[me, 0] = jnp.broadcast_to(own_sum, (rows, 128))
-    sums[me, 1] = jnp.broadcast_to(own_square, (rows, 128))
+    low_half = lax.broadcasted_iota(jnp.int32, (rows, 128), 1) < 64
+    sums[me] = jnp.where(low_half, own_sum, own_square)
     sum_copies = send_all(3, sums.at[me], sums.at[me])
     for copy in sum_copies:
         copy.wait_recv()
-    all_sum = functools.reduce(lambda a, b: a + b, [sums[p, 0] for p in range(group)])
-    all_square = functools.reduce(lambda a, b: a + b, [sums[p, 1] for p in range(group)])
-    mean = all_sum[:, :1] / width
-    var = all_square[:, :1] / width - mean * mean
+    all_sums = functools.reduce(lambda a, b: a + b, [sums[p] for p in range(group)])
+    mean = all_sums[:, :1] / width
+    var = all_sums[:, 64:65] / width - mean * mean
     gain = gout[:, pl.ds(pl.multiple_of(me * cols, cols), cols)]
     out_v[...] = ((summed - mean) * lax.rsqrt(var + 1e-05) * gain).astype(BF16)
 
@@ -306,7 +304,17 @@
             copy.wait_send()
     for _, _, copy in f_copies:
         copy.wait_send()
-    nst_store.wait()
+
+
+def store_kernel(out_v, nst_v, out_h, nst_h, sem):
+    copies = [
+        pltpu.make_async_copy(nst_v, nst_h, sem.at[0]),
+        pltpu.make_async_copy(out_v, out_h, sem.at[1]),
+    ]
+    for copy in copies:
+        copy.start()
+    for copy in copies:
+        copy.wait()
 
 
 def fused_step(
@@ -336,6 +344,7 @@
     inverse = np.tile(inverse.astype(np.float32), 2)[None, :]
     arrays = (
         tokens,
+        positions[None, :],
         state[0],
         w_query,
         w_key,
@@ -350,28 +359,28 @@
         jnp.asarray(inverse),
     )
     held = [pltpu.VMEM(a.shape, a.dtype) for a in arrays]
-    held.insert(2, pltpu.VMEM(arrays[1].shape, F32))
+    vmem_spec = pl.BlockSpec(memory_space=pltpu.VMEM)
     any_spec = pl.BlockSpec(memory_space=pl.ANY)
     out, new_state = pl.pallas_call(
         functools.partial(step_kernel, kv_count, tp_count),
         out_shape=(
-            jax.ShapeDtypeStruct((rows, cols), BF16),
-            jax.ShapeDtypeStruct(arrays[1].shape, F32),
+            pltpu.VMEM((rows, cols), BF16),
+            pltpu.VMEM(state.shape[1:], F32),
         ),
-        in_specs=[any_spec, pl.BlockSpec(memory_space=pltpu.SMEM)] + [any_spec] * 12,
-        out_specs=(pl.BlockSpec(memory_space=pltpu.VMEM), any_spec),
+        in_specs=[any_spec] * len(arrays),
+        out_specs=(vmem_spec, vmem_spec),
         scratch_shapes=held
         + [
             pltpu.VMEM((kv_count, 4, heads, width_head), F32),
             pltpu.VMEM((kv_count, 4, heads, width_head), F32),
             pltpu.VMEM((group * heads, width_head), F32),
-            pltpu.VMEM((group, rows, cols), F32),
+            pltpu.VMEM((group, rows, cols), BF16),
             pltpu.VMEM((group, rows, cols), F32),
             pltpu.VMEM((rows, width), BF16),
             pltpu.VMEM((rows, w_ffn_gate.shape[1]), BF16),
-            pltpu.VMEM((group, rows, cols), F32),
-            pltpu.VMEM((group, rows, cols), F32),
-            pltpu.VMEM((group, 2, rows, 128), F32),
+            pltpu.VMEM((group, rows, cols), BF16),
+            pltpu.VMEM((group, rows, cols), BF16),
+            pltpu.VMEM((group, rows, 128), F32),
             pltpu.SemaphoreType.DMA((len(arrays) + 1,)),
             pltpu.SemaphoreType.DMA((4, kv_count)),
             pltpu.SemaphoreType.DMA((4, kv_count)),
@@ -379,9 +388,20 @@
             pltpu.SemaphoreType.DMA((4, group)),
         ],
         compiler_params=pltpu.CompilerParams(
-            collective_id=0, has_side_effects=True, vmem_limit_bytes=60 * 1024 * 1024
+            collective_id=0, has_side_effects=True, vmem_limit_bytes=56 * 2**20
         ),
-    )(arrays[0], positions, *arrays[1:])
+    )(*arrays)
+    out, new_state = pl.pallas_call(
+        store_kernel,
+        out_shape=(
+            jax.ShapeDtypeStruct(out.shape, out.dtype),
+            jax.ShapeDtypeStruct(new_state.shape, new_state.dtype),
+        ),
+        in_specs=[vmem_spec, vmem_spec],
+        out_specs=(any_spec, any_spec),
+        scratch_shapes=[pltpu.SemaphoreType.DMA((2,))],
+        compiler_params=pltpu.CompilerParams(vmem_limit_bytes=2**20),
+    )(out, new_state)
     return out, new_state[None]
 
 

time: 41.1 us -> 37.3 us (0.908)
  local copies, waits for them, and re-layouts: 3.14 us -> 0 us
  Pallas kernels: 36.4 us -> 35.8 us
    unnamed x2 -> x0, local copies, waits for them, and re-layouts: 3.14 us -> none
    pallas_call x1, Pallas kernels: 36.4 us -> 35 us  [fused_step(): pl.pallas_call(functools.partial(step_kernel, kv_count, tp_count), out_sh...]
    pallas_call x0 -> x1, Pallas kernels: none -> 0.81 us  [fused_step(): pl.pallas_call(store_kernel, out_shape=(jax.ShapeDtypeStruct(out.shape, o...]
where the time goes in v2:
time: 37.3 us; the launch traced here: 37.1 us
  Pallas kernels  35.8 us (96%)
  between operations  1.29 us (3%)
    pallas_call x1, Pallas kernels, fused_step(): pl.pallas_call(functools.partial(step_kernel, kv_count, tp_count), out_sh...  35 us
    pallas_call x1, Pallas kernels, fused_step(): pl.pallas_call(store_kernel, out_shape=(jax.ShapeDtypeStruct(out.shape, o...  0.81 us

profile of v2, /device:TPU:0, one launch (start us, length us, event | category | flops | bytes accessed | tf_op | source)
XLA Modules:
  0.0 37.1 jit_solution(2988608308892870039)
XLA Ops:
  1.3 35.0 %shard_map.149 = (bf16[4,512]{1,0:T(4,128)(2,1)S(1)}, f32[8,128,128]{2,1,0:T(8,128)S(1)}) custom-call(bf16[4,1024]{1,0:T(4,128)(2,1)} %tok_h.1, s32[1,1]{1,0:T(1,128)} %bitcast.7.pos_h, f32[8,128,128]{2,1,0:T(8,128)} %bitcast.10, bf16[1024,1024]{1,0:T(8,128)(2,1)} %wq_h.1, bf16[1024,1024]{1,0:T(8,128)(2,1)} %wk_h.1, bf16[1024,1024]{1,0:T(8,128)(2,1)} %wv_h.1, ...), custom_call_target="tpu_custom_call" | custom-call | tf_op jit(solution)/shard_map/pallas_call | solution.py:364
  36.3 0.8 %shard_map.150 = (bf16[4,512]{1,0:T(4,128)(2,1)}, f32[8,128,128]{2,1,0:T(8,128)}) custom-call(bf16[4,512]{1,0:T(4,128)(2,1)S(1)} %get-tuple-element.6.out_v, f32[8,128,128]{2,1,0:T(8,128)S(1)} %get-tuple-element.7.nst_v), custom_call_target="tpu_custom_call" | custom-call | tf_op jit(solution)/shard_map/pallas_call | solution.py:394
